TPU v7x, 32 devices: a whole 2x2x4 slice. The times are simulated.
32 devices in a mesh: ep: 16 (over z, y, x), tp: 2 (over core).
Axes of the slice: x: 2, y: 2, z: 4, core: 2. Of those that a mesh axis runs over, the one named last changes fastest.
Arguments:
- tokens: bfloat16 [256, 1024], P('ep'), may hold values from -6 to 6
- mixer_gain: float32 [1024], replicated, may hold values from 0.1 to 1.9
- query_weight: bfloat16 [1024, 1024], P(None, 'tp'), may hold values from -0.1875 to 0.1875
- key_weight: bfloat16 [1024, 256], P(None, 'tp'), may hold values from -0.1875 to 0.1875
- value_weight: bfloat16 [1024, 256], P(None, 'tp'), may hold values from -0.1875 to 0.1875
- head_lambda: float32 [8], P('tp'), may hold values from 0.3 to 0.8
- head_gain: float32 [128], replicated, may hold values from 0.1 to 1.9
- out_weight: bfloat16 [1024, 1024], P('tp'), may hold values from -0.1875 to 0.1875
- cache_keys: bfloat16 [256, 1024, 256], P('ep', None, 'tp'), may hold values from -700 to 700
- cache_values: bfloat16 [256, 1024, 256], P('ep', None, 'tp'), may hold values from -6 to 6
- seq_lengths: int32 [256], P('ep'), may hold values from 2 to 1024, as said below
- channel_gain: float32 [1024], replicated, may hold values from 0.1 to 1.9
- expert_ids: int32 [256, 6], P('ep'), may hold values from 0 to 15, all different within a row; in each aligned block of 16 rows (0 to 15, 16 to 31, ...) at most 12 rows name the same one
- expert_shares: bfloat16 [256, 6], P('ep'), may hold values from 0.19921875 to 1
- expert_gate: bfloat16 [16, 1024, 256], P('ep', None, 'tp'), may hold values from -0.1875 to 0.1875
- expert_up: bfloat16 [16, 1024, 256], P('ep', None, 'tp'), may hold values from -0.1875 to 0.1875
- expert_down: bfloat16 [16, 256, 1024], P('ep', 'tp'), may hold values from -0.375 to 0.375
- dense_gate: bfloat16 [1024, 4096], P('tp', 'ep'), may hold values from -0.1875 to 0.1875
- dense_up: bfloat16 [1024, 4096], P('tp', 'ep'), may hold values from -0.1875 to 0.1875
- dense_down: bfloat16 [4096, 1024], P('ep', 'tp'), may hold values from -0.1875 to 0.1875
- branch_gate: float32 [1024], replicated, may hold values from -0.1875 to 0.1875
Outputs:
- layer_out: bfloat16 [256, 1024], P('ep', 'tp')
Inputs may be any that keep to these rules, and one draw needn't show every extreme that they name: `expert_ids`: each row names 6 different experts; among the 16 rows of one index of ep no expert is named by more than 12 rows. `seq_lengths`: some sequence has all 1024 positions live.
All inputs are finite; a program needn't handle non-finite values.
Results may differ from a plain program's by a relative error of at most 0.017.
The roundings to bfloat16 on the way count: a program that leaves them out, or rounds other values in their place, can miss the bound.
Values may be sent and summed in bfloat16 or wider, within the bound.
A program may use at most 64 MiB of HBM per device.

v0:
```python
import jax
import jax.numpy as jnp
from jax import lax
from jax.sharding import PartitionSpec as P

HD = 64


NORM_EPS = 1e-06
HEAD_EPS = 1e-05
THETA = 500000.0
LAMBDA_BASE = 0.2


def norm_rows(values, gain_vec, epsilon):
    mean_square = jnp.mean(values * values, axis=-1, keepdims=True)
    return values * lax.rsqrt(mean_square + epsilon) * gain_vec


def rotate(values, position):
    half_dim = HD // 2
    frequency = THETA ** (-jnp.arange(half_dim, dtype=jnp.float32) * (2.0 / HD))
    angles = position.astype(jnp.float32)[:, None] * frequency[None, :]
    cos_vals = jnp.cos(angles)[:, None, :]
    sin_vals = jnp.sin(angles)[:, None, :]
    first_half = values[..., :half_dim]
    second = values[..., half_dim:]
    return jnp.concatenate(
        [first_half * cos_vals - second * sin_vals, second * cos_vals + first_half * sin_vals],
        axis=-1,
    )


def expert_rows(arrived, expert_gate, expert_up, expert_down):
    source_count, slot_count, model_width = arrived.shape
    stacked = arrived.reshape(source_count * slot_count, model_width)
    gate_part = jnp.dot(stacked, expert_gate[0], preferred_element_type=jnp.float32)
    up_part = jnp.dot(stacked, expert_up[0], preferred_element_type=jnp.float32)
    expert_hidden = (jax.nn.silu(gate_part) * up_part).astype(jnp.bfloat16)
    partial_value = jnp.dot(expert_hidden, expert_down[0], preferred_element_type=jnp.float32)
    partial_value = partial_value.reshape(source_count, slot_count, model_width)
    return lax.psum_scatter(
        partial_value.astype(jnp.bfloat16), "tp", scatter_dimension=2, tiled=True
    )


def dense_branch(partials, dense_down):
    summed = lax.psum(partials.astype(jnp.bfloat16), "tp").astype(jnp.float32)
    unit_count = partials.shape[1] // 2
    dense_hidden = (jax.nn.silu(summed[:, :unit_count]) * summed[:, unit_count:]).astype(
        jnp.bfloat16
    )
    return jnp.dot(dense_hidden, dense_down, preferred_element_type=jnp.float32)


def shards(
    tokens,
    mixer_gain,
    query_weight,
    key_weight,
    value_weight,
    head_lambda,
    head_gain,
    out_weight,
    cache_keys,
    cache_values,
    seq_lengths,
    channel_gain,
    expert_ids,
    expert_shares,
    expert_gate,
    expert_up,
    expert_down,
    dense_gate,
    dense_up,
    dense_down,
    branch_gate,
):
    seq_count, model_width = tokens.shape
    resid = tokens.astype(jnp.float32)
    normed = norm_rows(resid, mixer_gain, NORM_EPS).astype(jnp.bfloat16)
    value_width = 2 * HD
    groups = cache_values.shape[2] // value_width
    local_heads = head_lambda.shape[0]
    per_group = local_heads // groups
    cache_span = cache_keys.shape[1]
    query_raw = jnp.dot(normed, query_weight, preferred_element_type=jnp.float32).reshape(
        seq_count, local_heads * 2, HD
    )
    key_raw = jnp.dot(normed, key_weight, preferred_element_type=jnp.float32).reshape(
        seq_count, groups * 2, HD
    )
    value_new = jnp.dot(normed, value_weight, preferred_element_type=jnp.float32).astype(
        jnp.bfloat16
    )
    value_new = value_new.reshape(seq_count, groups, value_width)
    query = (
        rotate(query_raw, seq_lengths)
        .astype(jnp.bfloat16)
        .reshape(seq_count, groups, per_group, 2, HD)
    )
    key_new = rotate(key_raw, seq_lengths).astype(jnp.bfloat16).reshape(seq_count, groups, 2, HD)
    key_rows = cache_keys.reshape(seq_count, cache_span, groups, 2, HD)
    value_rows = cache_values.reshape(seq_count, cache_span, groups, value_width)
    lambdas = head_lambda.reshape(groups, per_group)
    score_scale = HD ** (-0.5)
    scores = (
        jnp.einsum("sgjcd,slgcd->sgjcl", query, key_rows, preferred_element_type=jnp.float32)
        * score_scale
    )
    fresh_score = (
        jnp.einsum("sgjcd,sgcd->sgjc", query, key_new, preferred_element_type=jnp.float32)
        * score_scale
    )
    live = jnp.arange(cache_span)[None, :] < seq_lengths[:, None]
    scores = jnp.where(live[:, None, None, None, :], scores, -jnp.inf)
    peak = jnp.maximum(jnp.max(scores, axis=-1), fresh_score)
    expo_scores = jnp.exp(scores - peak[..., None])
    expo_fresh = jnp.exp(fresh_score - peak)
    denom_sum = jnp.sum(expo_scores, axis=-1) + expo_fresh
    probability = expo_scores / denom_sum[..., None]
    prob_fresh = expo_fresh / denom_sum
    weight = (probability[:, :, :, 0] - lambdas[None, :, :, None] * probability[:, :, :, 1]).astype(
        jnp.bfloat16
    )
    weight_fresh = (prob_fresh[..., 0] - lambdas[None] * prob_fresh[..., 1]).astype(jnp.bfloat16)
    head_mix = jnp.einsum("sgjl,slgv->sgjv", weight, value_rows, preferred_element_type=jnp.float32)
    head_mix = (
        head_mix
        + weight_fresh.astype(jnp.float32)[..., None] * value_new.astype(jnp.float32)[:, :, None, :]
    )
    head_mix = head_mix.reshape(seq_count, local_heads, value_width)
    head_out = (norm_rows(head_mix, head_gain, HEAD_EPS) * (1.0 - LAMBDA_BASE)).astype(jnp.bfloat16)
    attn_part = jnp.dot(
        head_out.reshape(seq_count, local_heads * value_width),
        out_weight,
        preferred_element_type=jnp.float32,
    )
    attn_sum = lax.psum(attn_part.astype(jnp.bfloat16), "tp").astype(jnp.float32)
    resid_mid = (resid + attn_sum).astype(jnp.bfloat16)
    ffn_input = norm_rows(resid_mid.astype(jnp.float32), channel_gain, NORM_EPS).astype(
        jnp.bfloat16
    )
    gate_own = jax.nn.sigmoid(
        jnp.dot(ffn_input.astype(jnp.float32), branch_gate, precision=lax.Precision.HIGHEST)
    )
    half_width = model_width // lax.axis_size("tp")
    offset = lax.axis_index("tp") * half_width
    mid_half = lax.dynamic_slice_in_dim(resid_mid, offset, half_width, 1)
    experts_total = lax.axis_size("ep")
    top_count = expert_ids.shape[1]
    capacity = max(2, 2 * seq_count * top_count // experts_total)
    slot_ids = jnp.arange(1, capacity + 1, dtype=jnp.int32)
    named_mask = expert_ids[:, :, None] == jnp.arange(experts_total, dtype=jnp.int32)[None, None, :]
    picked = jnp.any(named_mask, axis=1)
    share_wide = expert_shares.astype(jnp.float32)[:, :, None]
    row_share = jnp.sum(jnp.where(named_mask, share_wide, jnp.zeros_like(share_wide)), axis=1)
    slot_rank = jnp.cumsum(picked.astype(jnp.int32), axis=0)
    placed = picked[None, :, :] & (slot_rank[None, :, :] == slot_ids[:, None, None])
    outgoing = jnp.einsum(
        "cse,sd->ecd", placed.astype(jnp.bfloat16), ffn_input, preferred_element_type=jnp.float32
    ).astype(jnp.bfloat16)
    expert_out = expert_rows(
        lax.all_to_all(outgoing, "ep", split_axis=0, concat_axis=0, tiled=True),
        expert_gate,
        expert_up,
        expert_down,
    )
    returned = lax.all_to_all(expert_out, "ep", split_axis=0, concat_axis=0, tiled=True)
    routed_sum = jnp.einsum(
        "cse,ecd->sd",
        placed.astype(jnp.float32) * row_share[None],
        returned.astype(jnp.float32),
        precision=lax.Precision.HIGHEST,
    )
    input_half = lax.dynamic_slice_in_dim(ffn_input, offset, half_width, 1)
    piece_rows = lax.all_gather(input_half, "ep", axis=0, tiled=True)
    partials = jnp.concatenate(
        [
            jnp.dot(piece_rows, dense_gate, preferred_element_type=jnp.float32),
            jnp.dot(piece_rows, dense_up, preferred_element_type=jnp.float32),
        ],
        axis=1,
    )
    branch_term = dense_branch(partials, dense_down)
    summed = lax.psum_scatter(branch_term, "ep", scatter_dimension=0, tiled=True)
    summed = gate_own[:, None] * summed + routed_sum
    return (mid_half.astype(jnp.float32) + summed).astype(jnp.bfloat16)


def solution(mesh):
    placed = (
        P("ep", None),
        P(),
        P(None, "tp"),
        P(None, "tp"),
        P(None, "tp"),
        P("tp"),
        P(),
        P("tp", None),
        P("ep", None, "tp"),
        P("ep", None, "tp"),
        P("ep"),
        P(),
        P("ep", None),
        P("ep", None),
        P("ep", None, "tp"),
        P("ep", None, "tp"),
        P("ep", "tp", None),
        P("tp", "ep"),
        P("tp", "ep"),
        P("ep", "tp"),
        P(),
    )
    return jax.shard_map(
        shards, mesh=mesh, in_specs=placed, out_specs=P("ep", "tp"), check_vma=False
    )
```

profile of v0, /device:TPU:0, one launch (start us, length us, event | category | flops | bytes accessed | tf_op | source)
XLA Modules:
  0.0 203.1 jit_solution(3398508565920873563)
XLA Ops:
  6.5 0.7 convert_element_type.100
  7.3 0.7 iota_compare_fusion
  8.0 0.9 fusion.32
  8.9 1.2 fusion.59
  10.2 1.6 fusion.61
  12.6 6.4 %copy.65 = bf16[16,1024,128]{1,2,0:T(8,128)(2,1)} copy(bf16[16,1024,128]{2,1,0:T(8,128)(2,1)} %param.29) | data formatting | bytes 8388608 | tf_op args[8]
  19.1 3.0 %fusion.65 = (f32[16,4,2]{1,2,0:T(2,128)S(1)}, f32[16,1,4,2,1024]{4,2,3,0,1:T(4,128)S(1)}) fusion(bf16[16,1024,2,64]{1,3,2,0:T(8,128)(2,1)} %bitcast.151, bf16[16,4,2,32]{3,1,2,0:T(4,128)(2,1)S(1)} %copy.64, bf16[16,4,2,32]{3,1,2,0:T(4,128)(2,1)S(1)} %copy.63, pred[16,1024]{1,0:T(8,128)(4,1)S(1)} %iota_compare_fusion), kind=kOutput, calls=%fused_computation.106 | convolution fusion | flops 17203072 | bytes 4751872 | tf_op jit(solution)/shard_map/sgjcd,slgcd->sgjcl/dot_general | solution.py:108
  22.3 0.3 fusion.13
  22.9 0.3 fusion.12
  23.6 3.0 %multiply_reduce_fusion = (f32[16,4]{1,0:T(8,128)S(1)}, f32[16,4,128]{2,1,0:T(4,128)S(1)}) fusion(f32[16,128]{1,0:T(8,128)S(1)} %fusion.7, f32[16,4]{1,0:T(8,128)S(1)} %copy.71, bf16[16,1024,128]{2,1,0:T(8,128)(2,1)} %param.30, f32[16,1,4,2,1024]{4,2,3,0,1:T(4,128)S(1)} %fusion.12, f32[4]{0:T(128)S(1)} %copy-done.9), kind=kOutput, calls=%fused_computation.69 | convolution fusion | flops 17006528 | bytes 4760080 | tf_op jit(solution)/shard_map/sgjl,slgv->sgjv/dot_general | solution.py:127
  27.0 3.7 %psum.14 = bf16[16,1024]{1,0:T(8,128)(2,1)S(1)} all-reduce(bf16[16,1024]{1,0:T(8,128)(2,1)S(1)} %convolution_convert_fusion.3), channel_id=1, replica_groups=mesh['ep'=16,'tp'=2] {'tp'}, use_global_device_ids=true, to_apply=%region_4.5 | all-reduce | flops 16384 | bytes 65536 | tf_op jit(solution)/shard_map/psum | solution.py:139
  31.6 1.0 copy.73
  32.6 8.2 %all-to-all-start = ((bf16[16,12,1024]{2,1,0:T(8,128)(2,1)}), bf16[16,12,1024]{2,1,0:T(8,128)(2,1)S(1)}, u32[]{:S(2)}, u32[]{:S(2)}) async-start(bf16[16,12,1024]{2,1,0:T(8,128)(2,1)} %copy.73), calls=%async_computation.1 | async-start | bytes 1048576 | tf_op jit(solution)/shard_map/all_to_all | solution.py:164
  40.9 44.5 %all_gather.3 = bf16[256,512]{1,0:T(8,128)(2,1)S(1)} all-gather(bf16[16,512]{1,0:T(8,128)(2,1)S(1)} %constant_dynamic-slice_fusion), channel_id=1, replica_groups=mesh['ep'=16,'tp'=2] {'ep'}, dimensions={0}, use_global_device_ids=true | all-gather | bytes 278528 | tf_op jit(solution)/shard_map/all_gather | solution.py:177
  85.9 0.7 pad_maximum_fusion
  87.4 1.0 convolution_convert_fusion
  88.5 13.9 %all-reduce.2.cloned.1.call-done = bf16[256,512]{0,1:T(8,128)(2,1)} async-done(((bf16[256,512]{0,1:T(8,128)(2,1)}), bf16[256,512]{0,1:T(8,128)(2,1)}) %all-reduce.2.cloned.1.call-update) | async-done | bytes 262160 | tf_op jit(solution)/shard_map/psum | solution.py:48
  102.3 1.0 convert_element_type.112
  103.3 1.1 fusion.24
  104.4 9.2 %reduce-scatter.5.cloned.1.call-done = bf16[16,12,512]{2,0,1:T(8,128)(2,1)} async-done(((bf16[16,12,1024]{2,0,1:T(8,128)(2,1)}), bf16[16,12,512]{2,0,1:T(8,128)(2,1)}) %reduce-scatter.5.cloned.1.call-update) | async-done | bytes 196624 | tf_op jit(solution)/shard_map/reduce_scatter | solution.py:42
  113.7 1.7 copy.75
  115.4 6.7 %all-to-all-start.1 = ((bf16[16,12,512]{2,1,0:T(8,128)(2,1)}), bf16[16,12,512]{2,1,0:T(8,128)(2,1)S(1)}, u32[]{:S(2)}, u32[]{:S(2)}) async-start(bf16[16,12,512]{2,1,0:T(8,128)(2,1)} %copy.75), calls=%async_computation.3 | async-start | bytes 524288 | tf_op jit(solution)/shard_map/all_to_all | solution.py:169
  122.4 72.4 %reduce-scatter.3.cloned.1.call-done = f32[16,512]{1,0:T(8,128)} async-done(((f32[256,512]{1,0:T(8,128)}), f32[16,512]{1,0:T(8,128)}) %reduce-scatter.3.cloned.1.call-update) | async-done | bytes 32784 | tf_op jit(solution)/shard_map/reduce_scatter | solution.py:186
  194.8 1.8 fusion.6
  (87 shorter events, 4.5 us)
Async XLA Ops:
  6.5 20.2 %copy-start = (bf16[512,1024]{1,0:T(8,128)(2,1)S(1)}, bf16[512,1024]{1,0:T(8,128)(2,1)}, u32[]{:S(2)}) copy-start(bf16[512,1024]{1,0:T(8,128)(2,1)} %param.28) | copy-start | bytes 3145732
  19.1 4.1 %copy-start.9 = (f32[4]{0:T(128)S(1)}, f32[4]{0:T(128)}, u32[]{:S(2)}) copy-start(f32[4]{0:T(128)} %param.26) | copy-start | bytes 52
  19.1 4.3 %copy-start.1 = (bf16[16,1024]{1,0:T(8,128)(2,1)S(1)}, bf16[16,1024]{1,0:T(8,128)(2,1)}, u32[]{:S(2)}) copy-start(bf16[16,1024]{1,0:T(8,128)(2,1)} %param.21) | copy-start | bytes 98308
  19.1 4.3 %copy-start.7 = (f32[1024]{0:T(1024)S(1)}, f32[1024]{0:T(1024)}, u32[]{:S(2)}) copy-start(f32[1024]{0:T(1024)} %param.22) | copy-start | bytes 12292
  19.1 4.3 %copy-start.12 = (bf16[1024,128]{1,0:T(8,128)(2,1)S(1)}, bf16[1024,128]{1,0:T(8,128)(2,1)}, u32[]{:S(2)}) copy-start(bf16[1024,128]{1,0:T(8,128)(2,1)} %param.25) | copy-start | bytes 786436
  22.1 4.5 %copy-start.11 = (f32[128]{0:T(128)S(1)}, f32[128]{0:T(128)}, u32[]{:S(2)}) copy-start(f32[128]{0:T(128)} %param.27) | copy-start | bytes 1540
  22.1 8.8 %copy-start.6 = (s32[16,6]{0,1:T(8,128)S(1)}, s32[16,6]{0,1:T(8,128)}, u32[]{:S(2)}) copy-start(s32[16,6]{0,1:T(8,128)} %param.33) | copy-start | bytes 1156
  22.1 9.1 %copy-start.8 = (f32[1024]{0:T(1024)S(1)}, f32[1024]{0:T(1024)}, u32[]{:S(2)}) copy-start(f32[1024]{0:T(1024)} %param.32) | copy-start | bytes 12292
  23.6 61.8 %copy-start.3 = (bf16[512,256]{1,0:T(8,128)(2,1)S(1)}, bf16[512,256]{1,0:T(8,128)(2,1)}, u32[]{:S(2)}) copy-start(bf16[512,256]{1,0:T(8,128)(2,1)} %param.39) | copy-start | bytes 786436
  26.6 59.0 %copy-start.4 = (bf16[512,256]{1,0:T(8,128)(2,1)S(1)}, bf16[512,256]{1,0:T(8,128)(2,1)}, u32[]{:S(2)}) copy-start(bf16[512,256]{1,0:T(8,128)(2,1)} %param.38) | copy-start | bytes 786436
  26.7 60.1 %copy-start.2 = (bf16[1,1024,128]{2,1,0:T(8,128)(2,1)S(1)}, bf16[1,1024,128]{2,1,0:T(8,128)(2,1)}, u32[]{:S(2)}) copy-start(bf16[1,1024,128]{2,1,0:T(8,128)(2,1)} %param.35) | copy-start | bytes 786436
  30.7 56.4 %copy-start.13 = (bf16[1,1024,128]{2,1,0:T(8,128)(2,1)S(1)}, bf16[1,1024,128]{2,1,0:T(8,128)(2,1)}, u32[]{:S(2)}) copy-start(bf16[1,1024,128]{2,1,0:T(8,128)(2,1)} %param.36) | copy-start | bytes 786436
  31.6 55.8 %copy-start.5 = (bf16[1,128,1024]{2,1,0:T(8,128)(2,1)S(1)}, bf16[1,128,1024]{2,1,0:T(8,128)(2,1)}, u32[]{:S(2)}) copy-start(bf16[1,128,1024]{2,1,0:T(8,128)(2,1)} %param.37) | copy-start | bytes 786436
  32.6 70.7 %copy-start.14 = (bf16[256,512]{1,0:T(8,128)(2,1)S(1)}, bf16[256,512]{1,0:T(8,128)(2,1)}, u32[]{:S(2)}) copy-start(bf16[256,512]{1,0:T(8,128)(2,1)} %param.40) | copy-start | bytes 786436
  32.6 54.1 %all-to-all-start = ((bf16[16,12,1024]{2,1,0:T(8,128)(2,1)}), bf16[16,12,1024]{2,1,0:T(8,128)(2,1)S(1)}, u32[]{:S(2)}, u32[]{:S(2)}) async-start(bf16[16,12,1024]{2,1,0:T(8,128)(2,1)} %copy.73), calls=%async_computation.1 | async-start | bytes 1048576 | tf_op jit(solution)/shard_map/all_to_all | solution.py:164
  40.8 61.5 %all-reduce.2.cloned.1.call-start = ((), (), s32[]{:S(2)}) async-start(), calls=%async_computation.4 | async-start | bytes 524288 | tf_op jit(solution)/shard_map/psum | solution.py:48
  85.9 36.2 %copy-start.10 = (bf16[16,6]{0,1:T(8,128)(2,1)S(1)}, bf16[16,6]{0,1:T(8,128)(2,1)}, u32[]{:S(2)}) copy-start(bf16[16,6]{0,1:T(8,128)(2,1)} %param.34) | copy-start | bytes 580
  86.6 35.6 %copy-start.15 = (f32[1024]{0:T(1024)S(1)}, f32[1024]{0:T(1024)}, u32[]{:S(2)}) copy-start(f32[1024]{0:T(1024)} %param.41) | copy-start | bytes 12292
  86.7 27.0 %reduce-scatter.5.cloned.1.call-start = ((), (), s32[]{:S(2)}) async-start(), calls=%async_computation.6 | async-start | bytes 589824 | tf_op jit(solution)/shard_map/reduce_scatter | solution.py:42
  88.4 106.4 %reduce-scatter.3.cloned.1.call-start = ((), (), s32[]{:S(2)}) async-start(), calls=%async_computation.5 | async-start | bytes 557056 | tf_op jit(solution)/shard_map/reduce_scatter | solution.py:186
  115.4 79.4 %all-to-all-start.1 = ((bf16[16,12,512]{2,1,0:T(8,128)(2,1)}), bf16[16,12,512]{2,1,0:T(8,128)(2,1)S(1)}, u32[]{:S(2)}, u32[]{:S(2)}) async-start(bf16[16,12,512]{2,1,0:T(8,128)(2,1)} %copy.75), calls=%async_computation.3 | async-start | bytes 524288 | tf_op jit(solution)/shard_map/all_to_all | solution.py:169
Sparse Core Ops, SparseCore 0:
  86.8 15.5 all-reduce.1
  104.6 9.0 reduce-scatter.4
  115.9 78.8 reduce-scatter.2
where the time goes:
time: 204 us; the launch traced here: 203 us
  waiting for transfers between devices  95.6 us (47%)
  blocking collectives  48.2 us (24%)
  starting transfers between devices  15 us (7%)
  matrix products  14.8 us (7%)
  between operations  13.5 us (7%)
  local copies, waits for them, and re-layouts  10.3 us (5%)
  other arithmetic  5.81 us (3%)
    reduce_scatter x1, waiting for transfers between devices, shards(): lax.psum_scatter(branch_term, 'ep', scatter_dimension=0, tiled=True)  72.4 us
    all_gather x1, blocking collectives, shards(): piece_rows = lax.all_gather(input_half, 'ep', axis=0, tiled=True)  44.5 us
    psum x1, waiting for transfers between devices, dense_branch(): summed = lax.psum(partials.astype(jnp.bfloat16), 'tp').astype(jnp.float32)  13.9 us
    reduce_scatter x1, waiting for transfers between devices, expert_rows(): lax.psum_scatter(partial_value.astype(jnp.bfloat16), 'tp', scatter_dimens...  9.22 us
    all_to_all x1, starting transfers between devices, shards(): lax.all_to_all(outgoing, 'ep', split_axis=0, concat_axis=0, tiled=True)  8.15 us
    all_to_all x1, starting transfers between devices, shards(): lax.all_to_all(expert_out, 'ep', split_axis=0, concat_axis=0, tiled=True)  6.71 us
    unnamed x33, local copies, waits for them, and re-layouts  6.48 us
  transfers between devices with their start and end apart: 5, of which 3 were waited for; matrix products, arithmetic and copies ran while one was open for 3% of the time, Pallas kernels for 0%

commit v1 on v0

v1 whole, which is shorter than its diff:
```python
import functools

import jax
import jax.numpy as jnp
from jax import lax
from jax.experimental import pallas as pl
from jax.experimental.pallas import tpu as pltpu
from jax.sharding import PartitionSpec as P

HD = 64
NORM_EPS = 1e-06
HEAD_EPS = 1e-05
THETA = 500000.0
LAMBDA_BASE = 0.2
MESH = pl.DeviceIdType.MESH
F32 = jnp.float32
BF16 = jnp.bfloat16


def norm_rows(values, gain_vec, epsilon):
    mean_square = jnp.mean(values * values, axis=-1, keepdims=True)
    return values * lax.rsqrt(mean_square + epsilon) * gain_vec


def mm(a, b):
    return jnp.dot(a, b, preferred_element_type=F32)


def attend_kernel(
    heads, block, len_ref, lam_ref, tok_ref, gain_ref, wq_ref, wk_ref, wv_ref,
    cos_ref, sin_ref, hgain_ref, wo_ref, k_ref, v_ref, out_ref, q8, knew, vnew, mixed,
):
    step = pl.program_id(0)
    wide = 2 * HD
    seqs = tok_ref.shape[0]

    @pl.when(step == 0)
    def _():
        resid = tok_ref[...].astype(F32)
        normed = norm_rows(resid, gain_ref[...], NORM_EPS).astype(BF16)
        lane = lax.broadcasted_iota(jnp.int32, (seqs, wide), 1)
        first = (lane % HD) < HD // 2

        def rotate(x):
            swapped = jnp.where(
                first, pltpu.roll(x, wide - HD // 2, 1), pltpu.roll(x, HD // 2, 1)
            )
            return (x * cos_ref[...] + swapped * sin_ref[...]).astype(BF16).astype(F32)

        raw = mm(normed, wq_ref[...])
        for j in range(heads):
            rotated = rotate(raw[:, j * wide:(j + 1) * wide])
            q8[:, j, :] = jnp.where(lane < HD, rotated, 0.0)
            q8[:, heads + j, :] = jnp.where(lane < HD, 0.0, rotated)
        knew[...] = rotate(mm(normed, wk_ref[...]))
        vnew[...] = mm(normed, wv_ref[...]).astype(BF16).astype(F32)

    scale = HD ** (-0.5)
    span = k_ref.shape[1]
    position = lax.broadcasted_iota(jnp.int32, (2 * heads, span), 1)
    lam_rows = lax.broadcasted_iota(jnp.int32, (heads, 1), 0)
    lam = jnp.zeros((heads, 1), F32)
    for j in range(heads):
        lam = jnp.where(lam_rows == j, lam_ref[j], lam)
    for b in range(block):
        s = step * block + b
        query = q8[s]
        scores = lax.dot_general(
            query.astype(BF16), k_ref[b], (((1,), (1,)), ((), ())), preferred_element_type=F32
        ) * scale
        fresh = jnp.sum(query * knew[pl.ds(s, 1), :], axis=1, keepdims=True) * scale
        scores = jnp.where(position < len_ref[s], scores, -jnp.inf)
        peak = jnp.maximum(jnp.max(scores, axis=1, keepdims=True), fresh)
        expo = jnp.exp(scores - peak)
        expo_fresh = jnp.exp(fresh - peak)
        denom = jnp.sum(expo, axis=1, keepdims=True) + expo_fresh
        prob = expo / denom
        prob_fresh = expo_fresh / denom
        weight = (prob[:heads] - lam * prob[heads:]).astype(BF16)
        weight_fresh = (prob_fresh[:heads] - lam * prob_fresh[heads:]).astype(BF16).astype(F32)
        mix = mm(weight, v_ref[b]) + weight_fresh * vnew[pl.ds(s, 1), :]
        done = norm_rows(mix, hgain_ref[...], HEAD_EPS) * (1.0 - LAMBDA_BASE)
        for j in range(heads):
            mixed[j, pl.ds(s, 1), :] = done[j:j + 1]

    @pl.when(step == pl.num_programs(0) - 1)
    def _():
        rows = jnp.concatenate([mixed[j].astype(BF16) for j in range(heads)], axis=1)
        out_ref[...] = mm(rows, wo_ref[...])


def attend(tokens, mixer_gain, wq, wk, wv, head_lambda, head_gain, wo, keys, values, lengths):
    seqs, width = tokens.shape
    span = keys.shape[1]
    heads = head_lambda.shape[0]
    wide = 2 * HD
    block = 4 if seqs % 4 == 0 else 1
    half = HD // 2
    frequency = THETA ** (-jnp.arange(half, dtype=F32) * (2.0 / HD))
    angles = lengths.astype(F32)[:, None] * frequency[None, :]
    cos_vals = jnp.cos(angles)
    sin_vals = jnp.sin(angles)
    cos_wide = jnp.concatenate([cos_vals] * 4, axis=1)
    sin_wide = jnp.concatenate([-sin_vals, sin_vals] * 2, axis=1)

    def whole(x):
        return pl.BlockSpec(x.shape, lambda i: (0,) * x.ndim)

    smem = pl.BlockSpec(memory_space=pltpu.SMEM)
    gain2 = mixer_gain.reshape(1, -1)
    hgain2 = head_gain.reshape(1, -1)
    stream = pl.BlockSpec((block, span, wide), lambda i: (i, 0, 0))
    return pl.pallas_call(
        functools.partial(attend_kernel, heads, block),
        grid=(seqs // block,),
        out_shape=jax.ShapeDtypeStruct((seqs, width), F32),
        in_specs=[smem, smem, whole(tokens), whole(gain2), whole(wq), whole(wk), whole(wv),
                  whole(cos_wide), whole(sin_wide), whole(hgain2), whole(wo), stream, stream],
        out_specs=pl.BlockSpec((seqs, width), lambda i: (0, 0)),
        scratch_shapes=[
            pltpu.VMEM((seqs, 2 * heads, wide), F32),
            pltpu.VMEM((seqs, wide), F32),
            pltpu.VMEM((seqs, wide), F32),
            pltpu.VMEM((heads, seqs, wide), F32),
        ],
        compiler_params=pltpu.CompilerParams(dimension_semantics=("arbitrary",)),
        name="attend",
    )(lengths, head_lambda, tokens, gain2, wq, wk, wv, cos_wide, sin_wide, hgain2, wo, keys, values)


def ffn_kernel(
    n, parts, ids_ref, shares_ref, tok_ref, attn_ref, cgain_ref, bgate_ref,
    eg, eu, ed, dg, du, dd, out_ref,
    g, table, attn_in, egb, eub, edb, dgb, dub, ddb, pbuf, arrived,
    xsem, lsem, wsend, wrecv, shsend, shrecv, agsend, agrecv, fwsend, fwrecv, rssend, rsrecv,
):
    me = lax.axis_index("ep")
    t = lax.axis_index("tp")
    mate = 1 - t
    seqs, width = tok_ref.shape
    half = width // 2
    size = n // parts
    mine = me // size
    slot = me % size

    barrier = pltpu.get_barrier_semaphore()
    pl.semaphore_signal(barrier, inc=1, device_id=(me, mate), device_id_type=MESH)

    def greet(d, carry):
        pl.semaphore_signal(
            barrier, inc=1, device_id=((me + d) % n, t), device_id_type=MESH
        )
        return carry

    lax.fori_loop(1, n, greet, 0)

    fh = eg.shape[2]
    uh = dg.shape[0]
    own_cols = pl.ds(pl.multiple_of(t * fh, fh), fh)
    own_rows = pl.ds(pl.multiple_of(t * fh, fh), fh)
    own_feats = pl.ds(pl.multiple_of(t * uh, uh), uh)
    my_half = pl.ds(pl.multiple_of(t * half, half), half)
    mate_half = pl.ds(pl.multiple_of(mate * half, half), half)
    local = [
        (eg.at[0], egb.at[:, own_cols]),
        (eu.at[0], eub.at[:, own_cols]),
        (dg, dgb.at[own_feats, :]),
        (du, dub.at[own_feats, :]),
        (ed.at[0, :, my_half], edb.at[own_rows, :]),
        (dd, ddb),
    ]
    local = [pltpu.make_async_copy(a, b, lsem.at[i]) for i, (a, b) in enumerate(local)]
    for copy in local:
        copy.start()
    remote = [
        (eg.at[0], egb.at[:, own_cols]),
        (eu.at[0], eub.at[:, own_cols]),
        (dg, dgb.at[own_feats, :]),
        (du, dub.at[own_feats, :]),
        (ed.at[0, :, mate_half], edb.at[own_rows, :]),
    ]
    remote = [
        pltpu.make_async_remote_copy(a, b, wsend.at[i], wrecv.at[i],
                                     device_id=(me, mate), device_id_type=MESH)
        for i, (a, b) in enumerate(remote)
    ]

    lanes = table.shape[2]
    lane = lax.broadcasted_iota(jnp.int32, (seqs, lanes), 1)
    shares = jnp.zeros((seqs, lanes), F32)
    for k in range(ids_ref.shape[1]):
        shares += jnp.where(
            lane == ids_ref[:, k:k + 1], shares_ref[:, k:k + 1].astype(F32), 0.0
        )
    table[me] = shares.astype(BF16)

    pl.semaphore_wait(barrier, n)

    swap = pltpu.make_async_remote_copy(
        attn_ref, attn_in, xsem.at[0], xsem.at[1], device_id=(me, mate), device_id_type=MESH
    )
    swap.start()
    for copy in remote:
        copy.start()

    def to_peer(buffer, where, sends, recvs, peer):
        return pltpu.make_async_remote_copy(
            buffer.at[where], buffer.at[where], sends.at[peer], recvs.at[me],
            device_id=(peer, t), device_id_type=MESH,
        )

    def landed(buffer, where, sends, recvs, source):
        return pltpu.make_async_remote_copy(
            buffer.at[where], buffer.at[where], sends.at[source], recvs.at[source],
            device_id=(source, t), device_id_type=MESH,
        )

    def each(offset, visit):
        chunk = (mine + offset + parts) % parts

        def body(q, carry):
            peer = chunk * size + (slot + q) % size

            @pl.when(peer != me)
            def _():
                visit(peer)

            return carry

        lax.fori_loop(0, size, body, 0)
        return chunk

    for k in range(parts):
        each(-k, lambda peer: to_peer(table, me, shsend, shrecv, peer).start())

    swap.wait()
    attn_sum = attn_ref[...] + attn_in[...]
    mid = (tok_ref[...].astype(F32) + attn_sum).astype(BF16)
    wide_mid = mid.astype(F32)
    ffn_input = norm_rows(wide_mid, cgain_ref[...], NORM_EPS).astype(BF16)
    g[0, me] = ffn_input[:, :half]
    g[1, me] = ffn_input[:, half:]

    for k in range(parts):
        each(-k, lambda peer: to_peer(g, (t, me), agsend, agrecv, peer).start())

    def forward(source):
        return pltpu.make_async_remote_copy(
            g.at[t, source], g.at[t, source], fwsend.at[source], fwrecv.at[source],
            device_id=(me, mate), device_id_type=MESH,
        )

    def forwarded(source):
        return pltpu.make_async_remote_copy(
            g.at[mate, source], g.at[mate, source], fwsend.at[source], fwrecv.at[source],
            device_id=(me, mate), device_id_type=MESH,
        )

    def relay(source):
        landed(g, (t, source), agsend, agrecv, source).wait_recv()
        forward(source).start()

    def settle(source):
        forwarded(source).wait_recv()
        landed(table, source, shsend, shrecv, source).wait_recv()

    def send_back(peer):
        pltpu.make_async_remote_copy(
            pbuf.at[peer], arrived.at[me], rssend.at[peer], rsrecv.at[me],
            device_id=(peer, t), device_id_type=MESH,
        ).start()

    rows = size * seqs
    pick = lax.broadcasted_iota(jnp.int32, (rows, lanes), 1) == me
    for k in range(parts):
        chunk = each(k, relay)
        if k == 0:
            for copy in local:
                copy.wait()
            for copy in remote:
                copy.wait()
        each(k, settle)
        span = pl.ds(chunk * size, size)
        low = g[0, span].reshape(rows, half)
        high = g[1, span].reshape(rows, half)

        def product(weight):
            return mm(low, weight[:half]) + mm(high, weight[half:])

        gate_logit = jnp.sum(low.astype(F32) * bgate_ref[:, :half], axis=1, keepdims=True) + jnp.sum(
            high.astype(F32) * bgate_ref[:, half:], axis=1, keepdims=True
        )
        gate_value = jax.nn.sigmoid(gate_logit)
        share = jnp.sum(
            jnp.where(pick, table[span].reshape(rows, lanes).astype(F32), 0.0),
            axis=1, keepdims=True,
        )
        expert_hidden = (jax.nn.silu(product(egb)) * product(eub)).astype(BF16)
        expert_row = mm(expert_hidden, edb[...]).astype(BF16).astype(F32)
        dense_hidden = (jax.nn.silu(product(dgb)) * product(dub)).astype(BF16)
        dense_sum = mm(dense_hidden, ddb[...])
        total = (share * expert_row + gate_value * dense_sum).astype(BF16)
        pbuf[span] = total.reshape(size, seqs, half)
        each(k, send_back)

    arrived[me] = pbuf[me]
    for k in range(parts):
        each(-k, lambda peer: landed(arrived, peer, rssend, rsrecv, peer).wait_recv())

    result = lax.fori_loop(
        0, n, lambda i, acc: acc + arrived[i].astype(F32), jnp.zeros((seqs, half), F32)
    )
    mid_half = jnp.where(t == 0, wide_mid[:, :half], wide_mid[:, half:])
    out_ref[...] = (mid_half + result).astype(BF16)

    def drain(peer):
        to_peer(table, me, shsend, shrecv, peer).wait_send()
        to_peer(g, (t, me), agsend, agrecv, peer).wait_send()
        forward(peer).wait_send()
        pltpu.make_async_remote_copy(
            pbuf.at[peer], arrived.at[me], rssend.at[peer], rsrecv.at[me],
            device_id=(peer, t), device_id_type=MESH,
        ).wait_send()

    for k in range(parts):
        each(k, drain)


def ffn(n, ids, shares, tokens, attn, cgain, bgate, eg, eu, ed, dg, du, dd):
    seqs, width = tokens.shape
    half = width // 2
    lanes = -(-n // 128) * 128
    hidden = 2 * eg.shape[2]
    units = dg.shape[1]
    parts = 4 if n % 4 == 0 else 1
    vmem = pl.BlockSpec(memory_space=pltpu.VMEM)
    anyw = pl.BlockSpec(memory_space=pl.ANY)
    dma = pltpu.SemaphoreType.DMA
    return pl.pallas_call(
        functools.partial(ffn_kernel, n, parts),
        out_shape=jax.ShapeDtypeStruct((seqs, half), BF16),
        in_specs=[vmem] * 6 + [anyw] * 6,
        out_specs=vmem,
        scratch_shapes=[
            pltpu.VMEM((2, n, seqs, half), BF16),
            pltpu.VMEM((n, seqs, lanes), BF16),
            pltpu.VMEM((seqs, width), F32),
            pltpu.VMEM((width, hidden), BF16),
            pltpu.VMEM((width, hidden), BF16),
            pltpu.VMEM((hidden, half), BF16),
            pltpu.VMEM((width, units), BF16),
            pltpu.VMEM((width, units), BF16),
            pltpu.VMEM((units, half), BF16),
            pltpu.VMEM((n, seqs, half), BF16),
            pltpu.VMEM((n, seqs, half), BF16),
            dma((2,)), dma((6,)), dma((5,)), dma((5,)),
            dma((n,)), dma((n,)), dma((n,)), dma((n,)),
            dma((n,)), dma((n,)), dma((n,)), dma((n,)),
        ],
        compiler_params=pltpu.CompilerParams(collective_id=0, has_side_effects=True),
        name="ffn",
    )(ids, shares, tokens, attn, cgain.reshape(1, -1), bgate.reshape(1, -1), eg, eu, ed, dg, du, dd)


def shards(
    tokens, mixer_gain, query_weight, key_weight, value_weight, head_lambda, head_gain,
    out_weight, cache_keys, cache_values, seq_lengths, channel_gain, expert_ids,
    expert_shares, expert_gate, expert_up, expert_down, dense_gate, dense_up, dense_down,
    branch_gate,
):
    attn_part = attend(
        tokens, mixer_gain, query_weight, key_weight, value_weight, head_lambda, head_gain,
        out_weight, cache_keys, cache_values, seq_lengths,
    )
    return ffn(
        lax.axis_size("ep"), expert_ids, expert_shares, tokens, attn_part, channel_gain,
        branch_gate, expert_gate, expert_up, expert_down, dense_gate, dense_up, dense_down,
    )


def solution(mesh):
    placed = (
        P("ep", None), P(), P(None, "tp"), P(None, "tp"), P(None, "tp"), P("tp"), P(),
        P("tp", None), P("ep", None, "tp"), P("ep", None, "tp"), P("ep"), P(),
        P("ep", None), P("ep", None), P("ep", None, "tp"), P("ep", None, "tp"),
        P("ep", "tp", None), P("tp", "ep"), P("tp", "ep"), P("ep", "tp"), P(),
    )
    return jax.shard_map(
        shards, mesh=mesh, in_specs=placed, out_specs=P("ep", "tp"), check_vma=False
    )
```

time: 204 us -> 43 us (0.21)
  waiting for transfers between devices: 95.6 us -> 0 us
  blocking collectives: 48.2 us -> 0 us
  Pallas kernels: 0 us -> 36.9 us
  starting transfers between devices: 15 us -> 0 us
  matrix products: 14.8 us -> 0 us
  between operations: 13.5 us -> 0.02 us
  local copies, waits for them, and re-layouts: 10.3 us -> 4.04 us
  other arithmetic: 5.81 us -> 1.48 us
    reduce_scatter x2 -> x0, waiting for transfers between devices: 81.6 us -> none  [the longest x1 72.4 us: shards(): lax.psum_scatter(branch_term, 'ep', scatter_dimension=0, tiled=True)]
    all_gather x1 -> x0, blocking collectives: 44.5 us -> none  [shards(): piece_rows = lax.all_gather(input_half, 'ep', axis=0, tiled=True)]
    pallas_call x0 -> x2, Pallas kernels: none -> 36.9 us  [the longest x1 26.2 us: ffn(): pl.pallas_call(functools.partial(ffn_kernel, n, parts), out_shape=jax.Sha...]
    all_to_all x2 -> x0, starting transfers between devices: 14.9 us -> none  [the longest x1 8.15 us: shards(): lax.all_to_all(outgoing, 'ep', split_axis=0, concat_axis=0, tiled=True)]
    dot_general x15 -> x0, matrix products: 14.6 us -> none  [the longest x1 3.04 us: shards(): jnp.einsum('sgjcd,slgcd->sgjcl', query, key_rows, preferred_element_type=...]
    psum x1 -> x0, waiting for transfers between devices: 13.9 us -> none  [dense_branch(): summed = lax.psum(partials.astype(jnp.bfloat16), 'tp').astype(jnp.float32)]
    psum x1 -> x0, blocking collectives: 3.72 us -> none  [shards(): lax.psum(attn_part.astype(jnp.bfloat16), 'tp').astype(jnp.float32)]
    unnamed x33 -> x3, local copies, waits for them, and re-layouts: 6.48 us -> 4.04 us
  transfers between devices with their start and end apart: 5 -> 0, of which waited for: 3 -> 0; matrix products, arithmetic and copies ran while one was open for 3% -> 0% of each run, Pallas kernels for 0% -> 0%
where the time goes in v1:
time: 43 us; the launch traced here: 42.5 us
  Pallas kernels  36.9 us (86%)
  local copies, waits for them, and re-layouts  4.04 us (9%)
  other arithmetic  1.48 us (3%)
    pallas_call x1, Pallas kernels, ffn(): pl.pallas_call(functools.partial(ffn_kernel, n, parts), out_shape=jax.Sha...  26.2 us
    pallas_call x1, Pallas kernels, attend(): pl.pallas_call(functools.partial(attend_kernel, heads, block), grid=(seqs...  10.8 us
    unnamed x3, local copies, waits for them, and re-layouts  4.04 us

profile of v1, /device:TPU:0, one launch (start us, length us, event | category | flops | bytes accessed | tf_op | source)
XLA Modules:
  0.0 42.5 jit_solution(2682921930502249191)
XLA Ops:
  0.0 0.7 %convert_element_type.3 = f32[16]{0:T(128)S(1)} convert(s32[16]{0:T(128)} %len_ref.1) | non-fusion elementwise | flops 16 | bytes 128 | tf_op jit(solution)/shard_map/convert_element_type | solution.py:100
  0.7 1.4 %copy.23.shares_ref = bf16[16,6]{1,0:T(8,128)(2,1)} copy(bf16[16,6]{0,1:T(8,128)(2,1)} %param.34) | data formatting | bytes 384 | tf_op args[13]
  2.0 1.4 %copy.22.ids_ref = s32[16,6]{1,0:T(8,128)} copy(s32[16,6]{0,1:T(8,128)} %param.33) | data formatting | bytes 768 | tf_op args[12]
  3.4 0.1 fusion
  3.5 0.7 %pad_maximum_fusion = (f32[16,128]{1,0:T(8,128)}, f32[16,128]{1,0:T(8,128)}) fusion(f32[16,32]{1,0:T(8,128)S(1)} %get-tuple-element.7, f32[16,32]{1,0:T(8,128)S(1)} %get-tuple-element.6, f32[16,32]{1,0:T(8,128)S(1)} %get-tuple-element.5), kind=kLoop, calls=%fused_computation.2 | loop fusion | flops 12288 | bytes 22528 | tf_op jit(solution)/shard_map/concatenate | solution.py:103
  4.2 10.8 %attend.1.attn_ref = f32[16,1024]{1,0:T(8,128)} custom-call(s32[16]{0:T(128)} %len_ref.1, f32[4]{0:T(128)} %lam_ref.1, bf16[16,1024]{1,0:T(8,128)(2,1)} %tok_ref.3, f32[1,1024]{1,0:T(1,128)} %bitcast.4, bf16[1024,512]{1,0:T(8,128)(2,1)} %wq_ref.1, bf16[1024,128]{1,0:T(8,128)(2,1)} %wk_ref.1, bf16[1024,128]{1,0:T(8,128)(2,1)} %wv_ref.1, ...), custom_call_target="tpu_custom_call" | custom-call | tf_op jit(solution)/shard_map/attend/pallas_call | solution.py:113
  15.0 26.2 %ffn.1 = bf16[16,512]{1,0:T(8,128)(2,1)} custom-call(s32[16,6]{1,0:T(8,128)} %copy.22.ids_ref, bf16[16,6]{1,0:T(8,128)(2,1)} %copy.23.shares_ref, bf16[16,1024]{1,0:T(8,128)(2,1)} %tok_ref.3, f32[16,1024]{1,0:T(8,128)} %attend.1.attn_ref, f32[1,1024]{1,0:T(1,128)} %bitcast.5, f32[1,1024]{1,0:T(1,128)} %bitcast.6, bf16[1,1024,128]{2,1,0:T(8,128)(2,1)} %eg.1, ...), custom_call_target="tpu_custom_call" | custom-call | tf_op jit(solution)/shard_map/ffn/pallas_call | solution.py:339
  41.1 1.3 %copy.25 = bf16[16,512]{1,0:T(8,128)(2,1)} copy(bf16[16,512]{1,0:T(8,128)(2,1)} %ffn.1) | data formatting | bytes 32768
  (1 shorter events, 0.0 us)

commit v2 on v1

v2 whole, which is shorter than its diff:
```python
import functools

import jax
import jax.numpy as jnp
import numpy as np
from jax import lax
from jax.experimental import pallas as pl
from jax.experimental.pallas import tpu as pltpu
from jax.sharding import PartitionSpec as P

HD = 64
NORM_EPS = 1e-06
HEAD_EPS = 1e-05
THETA = 500000.0
LAMBDA_BASE = 0.2
TRIG_STEP = 32
MESH = pl.DeviceIdType.MESH
F32 = jnp.float32
BF16 = jnp.bfloat16


def norm_rows(values, gain_vec, epsilon):
    mean_square = jnp.mean(values * values, axis=-1, keepdims=True)
    return values * lax.rsqrt(mean_square + epsilon) * gain_vec


def mm(a, b):
    return jnp.dot(a, b, preferred_element_type=F32)


def layer_kernel(
    n, parts, block, len_ref, lam_ref, ids_ref, shares_ref, tok_ref, mgain_ref, hgain_ref,
    cgain_ref, bgate_ref, trig_ref, wq_hbm, wk_hbm, wv_hbm, wo_hbm, keys, values,
    eg, eu, ed, dg, du, dd, out_ref,
    wq, wk, wv, wo, kbuf, vbuf, trig, q8, knew, vnew, mixed, attn_ref,
    g, table, attn_in, egb, eub, edb, dgb, dub, ddb, pbuf, arrived,
    psem, ksem, vsem,
    xsem, lsem, wsend, wrecv, shsend, shrecv, agsend, agrecv, fwsend, fwrecv, rssend, rsrecv,
):
    me = lax.axis_index("ep")
    t = lax.axis_index("tp")
    mate = 1 - t
    seqs, width = tok_ref.shape
    half = width // 2
    size = n // parts
    mine = me // size
    slot = me % size

    seq_copies = [
        (
            pltpu.make_async_copy(keys.at[pl.ds(b, block)], kbuf.at[pl.ds(b, block)], ksem.at[b // block]),
            pltpu.make_async_copy(values.at[pl.ds(b, block)], vbuf.at[pl.ds(b, block)], vsem.at[b // block]),
        )
        for b in range(0, seqs, block)
    ]
    projections = [
        pltpu.make_async_copy(a, b, psem.at[i])
        for i, (a, b) in enumerate([(wq_hbm, wq), (wk_hbm, wk), (wv_hbm, wv), (wo_hbm, wo)])
    ]
    for copy in projections[:3]:
        copy.start()
    for pair in seq_copies:
        pair[0].start()
        pair[1].start()
    projections[3].start()

    barrier = pltpu.get_barrier_semaphore()
    pl.semaphore_signal(barrier, inc=1, device_id=(me, mate), device_id_type=MESH)

    def greet(d, carry):
        pl.semaphore_signal(
            barrier, inc=1, device_id=((me + d) % n, t), device_id_type=MESH
        )
        return carry

    lax.fori_loop(1, n, greet, 0)

    fh = eg.shape[2]
    uh = dg.shape[0]
    own_cols = pl.ds(pl.multiple_of(t * fh, fh), fh)
    own_rows = pl.ds(pl.multiple_of(t * fh, fh), fh)
    own_feats = pl.ds(pl.multiple_of(t * uh, uh), uh)
    my_half = pl.ds(pl.multiple_of(t * half, half), half)
    mate_half = pl.ds(pl.multiple_of(mate * half, half), half)
    local = [
        (eg.at[0], egb.at[:, own_cols]),
        (eu.at[0], eub.at[:, own_cols]),
        (dg, dgb.at[own_feats, :]),
        (du, dub.at[own_feats, :]),
        (ed.at[0, :, my_half], edb.at[own_rows, :]),
        (dd, ddb),
    ]
    local = [pltpu.make_async_copy(a, b, lsem.at[i]) for i, (a, b) in enumerate(local)]
    for copy in local:
        copy.start()
    remote = [
        (eg.at[0], egb.at[:, own_cols]),
        (eu.at[0], eub.at[:, own_cols]),
        (dg, dgb.at[own_feats, :]),
        (du, dub.at[own_feats, :]),
        (ed.at[0, :, mate_half], edb.at[own_rows, :]),
    ]
    remote = [
        pltpu.make_async_remote_copy(a, b, wsend.at[i], wrecv.at[i],
                                     device_id=(me, mate), device_id_type=MESH)
        for i, (a, b) in enumerate(remote)
    ]

    lanes = table.shape[2]
    named = lax.broadcasted_iota(jnp.int32, (lanes, seqs), 0)
    shares = jnp.zeros((lanes, seqs), F32)
    for k in range(ids_ref.shape[0]):
        shares += jnp.where(
            named == ids_ref[k:k + 1, :], shares_ref[k:k + 1, :].astype(F32), 0.0
        )
    table[me] = shares.T.astype(BF16)

    wide = 2 * HD
    heads = q8.shape[1] // 2
    for s in range(seqs):
        high = len_ref[s] // TRIG_STEP
        low = len_ref[s] % TRIG_STEP
        cos_h, sin_h = trig_ref[0, pl.ds(high, 1), :], trig_ref[1, pl.ds(high, 1), :]
        cos_l, sin_l = trig_ref[2, pl.ds(low, 1), :], trig_ref[3, pl.ds(low, 1), :]
        trig[0, pl.ds(s, 1), :] = cos_h * cos_l - sin_h * sin_l
        trig[1, pl.ds(s, 1), :] = sin_h * cos_l + cos_h * sin_l
    resid = tok_ref[...].astype(F32)
    normed = norm_rows(resid, mgain_ref[...], NORM_EPS).astype(BF16)
    qlane = lax.broadcasted_iota(jnp.int32, (seqs, wide), 1)
    first = (qlane % HD) < HD // 2
    cos_vals = trig[0]
    sin_vals = jnp.where(first, -trig[1], trig[1])

    def rotate(x):
        swapped = jnp.where(first, pltpu.roll(x, wide - HD // 2, 1), pltpu.roll(x, HD // 2, 1))
        return (x * cos_vals + swapped * sin_vals).astype(BF16).astype(F32)

    for copy in projections[:3]:
        copy.wait()
    raw = mm(normed, wq[...])
    for j in range(heads):
        rotated = rotate(raw[:, j * wide:(j + 1) * wide]) * HD ** (-0.5)
        q8[:, j, :] = jnp.where(qlane < HD, rotated, 0.0)
        q8[:, heads + j, :] = jnp.where(qlane < HD, 0.0, rotated)
    knew[...] = rotate(mm(normed, wk[...]))
    vnew[...] = mm(normed, wv[...]).astype(BF16).astype(F32)

    pl.semaphore_wait(barrier, n)
    for copy in remote:
        copy.start()

    def to_peer(buffer, where, sends, recvs, peer):
        return pltpu.make_async_remote_copy(
            buffer.at[where], buffer.at[where], sends.at[peer], recvs.at[me],
            device_id=(peer, t), device_id_type=MESH,
        )

    def landed(buffer, where, sends, recvs, source):
        return pltpu.make_async_remote_copy(
            buffer.at[where], buffer.at[where], sends.at[source], recvs.at[source],
            device_id=(source, t), device_id_type=MESH,
        )

    def each(offset, visit):
        chunk = (mine + offset + parts) % parts

        def body(q, carry):
            peer = chunk * size + (slot + q) % size

            @pl.when(peer != me)
            def _():
                visit(peer)

            return carry

        lax.fori_loop(0, size, body, 0)
        return chunk

    for k in range(parts):
        each(-k, lambda peer: to_peer(table, me, shsend, shrecv, peer).start())

    cached = kbuf.shape[1]
    tall = 2 * heads
    position = lax.broadcasted_iota(jnp.int32, (block, tall, cached), 2)
    which = lax.broadcasted_iota(jnp.int32, (block, tall, 1), 0)
    lam_rows = lax.broadcasted_iota(jnp.int32, (1, heads, 1), 1)
    lam = jnp.zeros((1, heads, 1), F32)
    for j in range(heads):
        lam = jnp.where(lam_rows == j, lam_ref[j], lam)
    for b0, (key_copy, value_copy) in zip(range(0, seqs, block), seq_copies):
        query = q8[b0:b0 + block]
        fresh = jnp.sum(query * knew[b0:b0 + block][:, None, :], axis=2, keepdims=True)
        live = jnp.zeros((block, tall, 1), jnp.int32)
        for b in range(block):
            live = jnp.where(which == b, len_ref[b0 + b], live)
        key_copy.wait()
        narrow = query.astype(BF16)
        scores = jnp.stack([
            lax.dot_general(narrow[b], kbuf[b0 + b], (((1,), (1,)), ((), ())),
                            preferred_element_type=F32)
            for b in range(block)
        ])
        scores = jnp.where(position < live, scores, -jnp.inf)
        peak = jnp.maximum(jnp.max(scores, axis=2, keepdims=True), fresh)
        expo = jnp.exp(scores - peak)
        expo_fresh = jnp.exp(fresh - peak)
        inverse = 1.0 / (jnp.sum(expo, axis=2, keepdims=True) + expo_fresh)
        prob_fresh = expo_fresh * inverse
        weight = (
            expo[:, :heads] * inverse[:, :heads] - expo[:, heads:] * (lam * inverse[:, heads:])
        ).astype(BF16)
        weight_fresh = (prob_fresh[:, :heads] - lam * prob_fresh[:, heads:]).astype(BF16).astype(F32)
        value_copy.wait()
        mix = jnp.stack([mm(weight[b], vbuf[b0 + b]) for b in range(block)])
        mix = mix + weight_fresh * vnew[b0:b0 + block][:, None, :]
        done = norm_rows(mix, hgain_ref[...], HEAD_EPS) * (1.0 - LAMBDA_BASE)
        for b in range(block):
            for j in range(heads):
                mixed[j, b0 + b:b0 + b + 1, :] = done[b, j:j + 1]
    projections[3].wait()
    rows = jnp.concatenate([mixed[j].astype(BF16) for j in range(heads)], axis=1)
    attn_ref[...] = mm(rows, wo[...])
    swap = pltpu.make_async_remote_copy(
        attn_ref, attn_in, xsem.at[0], xsem.at[1], device_id=(me, mate), device_id_type=MESH
    )
    swap.start()

    swap.wait()
    attn_sum = attn_ref[...] + attn_in[...]
    mid = (tok_ref[...].astype(F32) + attn_sum).astype(BF16)
    wide_mid = mid.astype(F32)
    ffn_input = norm_rows(wide_mid, cgain_ref[...], NORM_EPS).astype(BF16)
    g[0, me] = ffn_input[:, :half]
    g[1, me] = ffn_input[:, half:]

    for k in range(parts):
        each(-k, lambda peer: to_peer(g, (t, me), agsend, agrecv, peer).start())

    def forward(source):
        return pltpu.make_async_remote_copy(
            g.at[t, source], g.at[t, source], fwsend.at[source], fwrecv.at[source],
            device_id=(me, mate), device_id_type=MESH,
        )

    def forwarded(source):
        return pltpu.make_async_remote_copy(
            g.at[mate, source], g.at[mate, source], fwsend.at[source], fwrecv.at[source],
            device_id=(me, mate), device_id_type=MESH,
        )

    def relay(source):
        landed(g, (t, source), agsend, agrecv, source).wait_recv()
        forward(source).start()

    def settle(source):
        forwarded(source).wait_recv()
        landed(table, source, shsend, shrecv, source).wait_recv()

    def send_back(peer):
        pltpu.make_async_remote_copy(
            pbuf.at[peer], arrived.at[me], rssend.at[peer], rsrecv.at[me],
            device_id=(peer, t), device_id_type=MESH,
        ).start()

    rows = size * seqs
    pick = lax.broadcasted_iota(jnp.int32, (rows, lanes), 1) == me
    for k in range(parts):
        chunk = each(k, relay)
        if k == 0:
            for copy in local:
                copy.wait()
            for copy in remote:
                copy.wait()
        each(k, settle)
        span = pl.ds(chunk * size, size)
        low = g[0, span].reshape(rows, half)
        high = g[1, span].reshape(rows, half)

        def product(weight):
            return mm(low, weight[:half]) + mm(high, weight[half:])

        gate_logit = jnp.sum(low.astype(F32) * bgate_ref[:, :half], axis=1, keepdims=True) + jnp.sum(
            high.astype(F32) * bgate_ref[:, half:], axis=1, keepdims=True
        )
        gate_value = jax.nn.sigmoid(gate_logit)
        share = jnp.sum(
            jnp.where(pick, table[span].reshape(rows, lanes).astype(F32), 0.0),
            axis=1, keepdims=True,
        )
        expert_hidden = (jax.nn.silu(product(egb)) * product(eub)).astype(BF16)
        expert_row = mm(expert_hidden, edb[...]).astype(BF16).astype(F32)
        dense_hidden = (jax.nn.silu(product(dgb)) * product(dub)).astype(BF16)
        dense_sum = mm(dense_hidden, ddb[...])
        total = (share * expert_row + gate_value * dense_sum).astype(BF16)
        pbuf[span] = total.reshape(size, seqs, half)
        each(k, send_back)

    arrived[me] = pbuf[me]
    for k in range(parts):
        each(-k, lambda peer: landed(arrived, peer, rssend, rsrecv, peer).wait_recv())

    result = lax.fori_loop(
        0, n, lambda i, acc: acc + arrived[i].astype(F32), jnp.zeros((seqs, half), F32)
    )
    mid_half = jnp.where(t == 0, wide_mid[:, :half], wide_mid[:, half:])
    out_ref[...] = mid_half + result

    def drain(peer):
        to_peer(table, me, shsend, shrecv, peer).wait_send()
        to_peer(g, (t, me), agsend, agrecv, peer).wait_send()
        forward(peer).wait_send()
        pltpu.make_async_remote_copy(
            pbuf.at[peer], arrived.at[me], rssend.at[peer], rsrecv.at[me],
            device_id=(peer, t), device_id_type=MESH,
        ).wait_send()

    for k in range(parts):
        each(k, drain)


def trig_tables(cached):
    frequency = THETA ** (-np.arange(HD // 2, dtype=np.float32) * np.float32(2.0 / HD))
    frequency = np.tile(frequency.astype(np.float32).astype(np.float64), 4)
    rows = max(cached // TRIG_STEP + 1, TRIG_STEP)
    rows = -(-rows // 8) * 8
    high = (np.arange(rows) * TRIG_STEP)[:, None] * frequency[None]
    low = np.arange(rows)[:, None] * frequency[None]
    return np.stack([np.cos(high), np.sin(high), np.cos(low), np.sin(low)]).astype(np.float32)


def shards(
    tokens, mixer_gain, query_weight, key_weight, value_weight, head_lambda, head_gain,
    out_weight, cache_keys, cache_values, seq_lengths, channel_gain, expert_ids,
    expert_shares, expert_gate, expert_up, expert_down, dense_gate, dense_up, dense_down,
    branch_gate,
):
    n = lax.axis_size("ep")
    seqs, width = tokens.shape
    half = width // 2
    heads = head_lambda.shape[0]
    wide = 2 * HD
    block = 4 if seqs % 4 == 0 else 1
    lanes = -(-n // 128) * 128
    hidden = 2 * expert_gate.shape[2]
    units = dense_gate.shape[1]
    parts = 4 if n % 4 == 0 else 1
    vmem = pl.BlockSpec(memory_space=pltpu.VMEM)
    smem = pl.BlockSpec(memory_space=pltpu.SMEM)
    anyw = pl.BlockSpec(memory_space=pl.ANY)
    dma = pltpu.SemaphoreType.DMA
    trig = jnp.asarray(trig_tables(cache_keys.shape[1]))
    out = pl.pallas_call(
        functools.partial(layer_kernel, n, parts, block),
        out_shape=jax.ShapeDtypeStruct((seqs, half), F32),
        in_specs=[smem] * 2 + [vmem] * 8 + [anyw] * 12,
        out_specs=vmem,
        scratch_shapes=[
            pltpu.VMEM(query_weight.shape, BF16),
            pltpu.VMEM(key_weight.shape, BF16),
            pltpu.VMEM(value_weight.shape, BF16),
            pltpu.VMEM(out_weight.shape, BF16),
            pltpu.VMEM(cache_keys.shape, BF16),
            pltpu.VMEM(cache_values.shape, BF16),
            pltpu.VMEM((2, seqs, wide), F32),
            pltpu.VMEM((seqs, 2 * heads, wide), F32),
            pltpu.VMEM((seqs, wide), F32),
            pltpu.VMEM((seqs, wide), F32),
            pltpu.VMEM((heads, seqs, wide), F32),
            pltpu.VMEM((seqs, width), F32),
            pltpu.VMEM((2, n, seqs, half), BF16),
            pltpu.VMEM((n, seqs, lanes), BF16),
            pltpu.VMEM((seqs, width), F32),
            pltpu.VMEM((width, hidden), BF16),
            pltpu.VMEM((width, hidden), BF16),
            pltpu.VMEM((hidden, half), BF16),
            pltpu.VMEM((width, units), BF16),
            pltpu.VMEM((width, units), BF16),
            pltpu.VMEM((units, half), BF16),
            pltpu.VMEM((n, seqs, half), BF16),
            pltpu.VMEM((n, seqs, half), BF16),
            dma((4,)), dma((seqs // block,)), dma((seqs // block,)),
            dma((2,)), dma((6,)), dma((5,)), dma((5,)),
            dma((n,)), dma((n,)), dma((n,)), dma((n,)),
            dma((n,)), dma((n,)), dma((n,)), dma((n,)),
        ],
        compiler_params=pltpu.CompilerParams(collective_id=0, has_side_effects=True),
        name="layer",
    )(
        seq_lengths, head_lambda, expert_ids.T, expert_shares.T, tokens,
        mixer_gain.reshape(1, -1), head_gain.reshape(1, -1), channel_gain.reshape(1, -1),
        branch_gate.reshape(1, -1), trig, query_weight, key_weight, value_weight, out_weight,
        cache_keys, cache_values, expert_gate, expert_up, expert_down,
        dense_gate, dense_up, dense_down,
    )
    return out.astype(BF16)


def solution(mesh):
    placed = (
        P("ep", None), P(), P(None, "tp"), P(None, "tp"), P(None, "tp"), P("tp"), P(),
        P("tp", None), P("ep", None, "tp"), P("ep", None, "tp"), P("ep"), P(),
        P("ep", None), P("ep", None), P("ep", None, "tp"), P("ep", None, "tp"),
        P("ep", "tp", None), P("tp", "ep"), P("tp", "ep"), P("ep", "tp"), P(),
    )
    return jax.shard_map(
        shards, mesh=mesh, in_specs=placed, out_specs=P("ep", "tp"), check_vma=False
    )
```

time: 43 us -> 32.2 us (0.75)
  Pallas kernels: 36.9 us -> 30.6 us
  local copies, waits for them, and re-layouts: 4.04 us -> 0 us
    pallas_call x2 -> x1, Pallas kernels: 36.9 us -> 30.6 us  [shards(): pl.pallas_call(functools.partial(layer_kernel, n, parts, block), out_shap...]
    unnamed x3 -> x0, local copies, waits for them, and re-layouts: 4.04 us -> none
    convert_element_type x1, other arithmetic: 0.66 us -> 1.37 us  [shards(): return out.astype(BF16)]
    concatenate x1 -> x0, other arithmetic: 0.69 us -> none  [attend(): cos_wide = jnp.concatenate([cos_vals] * 4, axis=1)]
where the time goes in v2:
time: 32.2 us; the launch traced here: 32 us
  Pallas kernels  30.6 us (95%)
  other arithmetic  1.37 us (4%)
    pallas_call x1, Pallas kernels, shards(): pl.pallas_call(functools.partial(layer_kernel, n, parts, block), out_shap...  30.6 us
    convert_element_type x1, other arithmetic, shards(): return out.astype(BF16)  1.37 us

profile of v2, /device:TPU:0, one launch (start us, length us, event | category | flops | bytes accessed | tf_op | source)
XLA Modules:
  0.0 32.0 jit_solution(3044470351498863248)
XLA Ops:
  0.0 30.6 %layer.1 = f32[16,512]{1,0:T(8,128)} custom-call(s32[16]{0:T(128)} %len_ref.1, f32[4]{0:T(128)} %lam_ref.1, s32[6,16]{1,0:T(8,128)} %bitcast.6, bf16[6,16]{1,0:T(8,128)(2,1)} %bitcast.10, bf16[16,1024]{1,0:T(8,128)(2,1)} %tok_ref.1, f32[1,1024]{1,0:T(1,128)} %bitcast.7, f32[1,128]{1,0:T(1,128)} %bitcast.11, f32[1,1024]{1,0:T(1,128)} %bitcast.8, ...), custom_call_target="tpu_custom_call" | custom-call | tf_op jit(solution)/shard_map/layer/pallas_call | solution.py:352
  30.6 1.4 %convert_element_type.3 = bf16[16,512]{1,0:T(8,128)(2,1)} convert(f32[16,512]{1,0:T(8,128)} %layer.1) | non-fusion elementwise | flops 8192 | bytes 49152 | tf_op jit(solution)/shard_map/convert_element_type | solution.py:395
